TPU v7x, 32 devices: a whole 2x2x4 slice. The times are simulated.
32 devices in a mesh: gr: 2 (over x), sp: 8 (over z, y), tp: 2 (over core).
Axes of the slice: x: 2, y: 2, z: 4, core: 2. Of those that a mesh axis runs over, the one named last changes fastest.
Arguments:
- tokens: bfloat16 [8, 1536, 2048], P('gr', 'sp'), parts along dimension 0, may hold values from -6 to 6
- key_weight: bfloat16 [2048, 512], P(None, 'tp'), may hold values from -0.125 to 0.125
- value_weight: bfloat16 [2048, 1024], P(None, 'tp'), may hold values from -0.125 to 0.125
- input_weight: bfloat16 [2048, 8], P(None, 'tp'), may hold values from -0.125 to 0.125
- forget_weight: bfloat16 [2048, 8], P(None, 'tp'), may hold values from -0.125 to 0.125
- forget_bias: float32 [8], P('tp'), may hold values from 2.5 to 9.5
- query: bfloat16 [8, 512], P('gr', 'tp'), parts along dimension 0, may hold values from -6 to 6
Outputs:
- key_cache: bfloat16 [16, 768, 512], P(('gr', 'sp'), None, 'tp'), parts along dimension 0
- value_cache: bfloat16 [16, 768, 1024], P(('gr', 'sp'), None, 'tp'), parts along dimension 0
- memory: float32 [8, 8, 64, 128], P('gr', 'tp'), parts along dimension 0
- normalizer: float32 [8, 8, 64], P('gr', 'tp'), parts along dimension 0
- stabilizer: float32 [8, 8], P('gr', 'tp'), parts along dimension 0
- first_read: float32 [8, 1024], P('gr', 'tp'), parts along dimension 0
There are 2 independent parts, one for each index of `gr`. A program takes and returns all parts, laid end to end along the dimension named above; an argument that names none is the same for every part. Nothing has to cross between parts.
All inputs are finite; a program needn't handle non-finite values.
Results may differ from a plain program's by a relative error of at most 0.0015.
The roundings to bfloat16 on the way count: a program that leaves them out, or rounds other values in their place, can miss the bound.
Values may be sent and summed in bfloat16 or wider, within the bound.
A program may use at most 64 MiB of HBM per device.

v0:
```python
import jax
import jax.numpy as jnp
from jax import lax
from jax.sharding import PartitionSpec as P


def carried_in(array, axis, combine, identity):
    size, index = (lax.axis_size(axis), lax.axis_index(axis))
    everything = lax.all_gather(array, axis)
    start = jnp.broadcast_to(jnp.asarray(identity, array.dtype), array.shape)

    def step(k, before):
        at = size - 1 - k
        reached = at > index
        new = combine(before, everything[at])
        return jnp.where(reached, new, before)

    return lax.fori_loop(0, size, step, start)


def merged(value, axis, join):
    pieces = jax.tree.map(lambda part: lax.all_gather(part, axis), value)
    head = jax.tree.map(lambda part: part[0], pieces)
    tail = jax.tree.map(lambda part: part[1:], pieces)
    so_far, _ = lax.scan(lambda so_far, share: (join(so_far, share), None), head, tail)
    return so_far


def add_pair(earlier, later):
    return earlier + later


def block_state(keys3, values3, igate, logf, later, kdim):
    seqs, span, heads = logf.shape
    total = jnp.sum(logf, axis=1)
    logw = (later + total)[:, None, :] - jnp.cumsum(logf, axis=1) + igate
    top = jnp.max(logw, axis=1)
    weight = jnp.exp(logw - top[:, None, :]) * kdim ** (-0.5)
    keys4 = keys3.reshape(seqs, span, heads, kdim).astype(jnp.float32)
    values4 = values3.reshape(seqs, span, heads, -1).astype(jnp.float32)
    scaled = keys4 * weight[..., None]
    memory = jnp.einsum("slhd,slhe->shde", scaled, values4, precision=lax.Precision.HIGHEST)
    return (memory, jnp.sum(scaled, axis=1), top, total)


def merge_states(first, second):
    top = jnp.maximum(first[2], second[2])
    left = jnp.exp(first[2] - top)
    right = jnp.exp(second[2] - top)
    memory = first[0] * left[..., None, None] + second[0] * right[..., None, None]
    normal = first[1] * left[..., None] + second[1] * right[..., None]
    return (memory, normal, top, first[3] + second[3])


def local(tokens, key_weight, value_weight, input_weight, forget_weight, forget_bias, query):
    seqs, span, width = tokens.shape
    heads = input_weight.shape[1]
    kdim = key_weight.shape[1] // heads
    vdim = value_weight.shape[1] // heads
    pieces = lax.axis_size("sp") // seqs
    sub = span // pieces
    flat = tokens.reshape(seqs * span, width)
    keys = jnp.dot(flat, key_weight, preferred_element_type=jnp.float32).astype(jnp.bfloat16)
    values = jnp.dot(flat, value_weight, preferred_element_type=jnp.float32).astype(jnp.bfloat16)
    gate_pair = jnp.concatenate([input_weight, forget_weight], axis=1)
    gates = jnp.dot(flat, gate_pair, preferred_element_type=jnp.float32)
    igate = gates[:, :heads].reshape(seqs, span, heads)
    logf = jax.nn.log_sigmoid(gates[:, heads:] + forget_bias).reshape(seqs, span, heads)
    keys3 = keys.reshape(seqs, span, heads * kdim)
    values3 = values.reshape(seqs, span, heads * vdim)
    key_cache, value_cache = (
        lax.all_to_all(
            keys3.reshape(seqs * pieces, sub, heads * kdim),
            "sp",
            split_axis=0,
            concat_axis=1,
            tiled=True,
        ),
        lax.all_to_all(
            values3.reshape(seqs * pieces, sub, heads * vdim),
            "sp",
            split_axis=0,
            concat_axis=1,
            tiled=True,
        ),
    )
    zeros = jnp.zeros((seqs, heads), jnp.float32)
    later = carried_in(jnp.sum(logf, axis=1), "sp", add_pair, zeros)
    memory_part, normal_part, top, total = block_state(keys3, values3, igate, logf, later, kdim)
    memory_all, normal_all, top_all, total_all = merged(
        (memory_part, normal_part, top, total), "sp", merge_states
    )
    stabilizer = jnp.maximum(top_all, total_all)
    factor = jnp.exp(top_all - stabilizer)
    memory = memory_all * factor[..., None, None]
    normalizer = normal_all * factor[..., None]
    asked = query.astype(jnp.float32).reshape(query.shape[0], heads, kdim)
    numer = jnp.einsum("shd,shde->she", asked, memory, precision=lax.Precision.HIGHEST)
    denom = jnp.maximum(jnp.abs(jnp.sum(asked * normalizer, axis=-1)), 1.0)
    first_read = (numer / denom[..., None]).reshape(query.shape[0], heads * vdim)
    return (key_cache, value_cache, memory, normalizer, stabilizer, first_read)


def solution(mesh):
    return jax.shard_map(
        local,
        mesh=mesh,
        in_specs=(
            P("gr", "sp", None),
            P(None, "tp"),
            P(None, "tp"),
            P(None, "tp"),
            P(None, "tp"),
            P("tp"),
            P("gr", "tp"),
        ),
        out_specs=(
            P(("gr", "sp"), None, "tp"),
            P(("gr", "sp"), None, "tp"),
            P("gr", "tp", None, None),
            P("gr", "tp", None),
            P("gr", "tp"),
            P("gr", "tp"),
        ),
        check_vma=False,
    )
```

profile of v0, /device:TPU:0, one launch (start us, length us, event | category | flops | bytes accessed | tf_op | source)
XLA Modules:
  0.0 211.6 jit_solution(7671632423110484531)
XLA Ops:
  7.2 1.8 copy-done
  9.1 2.4 %convolution_convert_fusion.1 = bf16[768,256]{1,0:T(8,128)(2,1)S(1)} fusion(bf16[768,2048]{1,0:T(8,128)(2,1)S(1)} %bitcast.70, bf16[2048,256]{1,0:T(8,128)(2,1)} %param.12), kind=kOutput, calls=%fused_computation.11 | convolution fusion | flops 805502976 | bytes 4587520 | tf_op jit(solution)/shard_map/dot_general | solution.py:63
  11.4 2.7 %convolution_convert_fusion = bf16[768,512]{1,0:T(8,128)(2,1)} fusion(bf16[768,2048]{1,0:T(8,128)(2,1)S(1)} %bitcast.71, bf16[2048,512]{1,0:T(8,128)(2,1)S(1)} %copy-done.6), kind=kOutput, calls=%fused_computation.10 | convolution fusion | flops 1611005952 | bytes 6029312 | tf_op jit(solution)/shard_map/dot_general | solution.py:64
  14.1 1.1 copy.31
  15.2 2.8 %reshape.70 = f32[4,192,4,64]{1,0,3,2:T(4,128)} reshape(f32[768,256]{0,1:T(8,128)} %copy.31) | data formatting | bytes 1572864 | tf_op jit(solution)/shard_map/convert_element_type | solution.py:39
  18.1 1.6 convolution_bitcast_fusion
  20.1 4.8 %reduce-window.6 = f32[4,4,2,128]{3,2,1,0:T(2,128)S(1)} reduce-window(f32[4,4,2,128]{3,2,1,0:T(2,128)S(1)} %copy.34, f32[]{:T(128)} %constant.71.clone.1), window={size=1x1x1x128 pad=0_0x0_0x0_0x127_0}, to_apply=%region_3.4 | reduce-window | flops 520192 | bytes 32772 | tf_op jit(solution)/shard_map/reduce-window
  25.1 0.1 copy.35
  25.2 0.1 copy.36
  25.6 27.9 %all-gather.4 = f32[8,4,4]{2,1,0:T(4,128)S(1)} all-gather(f32[1,4,4]{2,1,0:T(4,128)S(1)} %bitcast.83), channel_id=2, replica_groups=mesh['gr'=2,'sp'=8,'tp'=2] {'sp'}, dimensions={0}, use_global_device_ids=true | all-gather | bytes 576 | tf_op jit(solution)/shard_map/all_gather | solution.py:9
  53.5 0.3 while.33
  53.9 0.2 fusion.14
  54.2 2.4 %reshape_reshape.12 = bf16[4,192,4,128]{3,2,1,0:T(4,128)(2,1)} reshape(bf16[768,512]{1,0:T(8,128)(2,1)} %convolution_convert_fusion) | data formatting | bytes 1572864 | tf_op jit(solution)/shard_map/reshape;reshape | solution.py:40
  56.6 2.3 %fusion.16 = (f32[4,4,64]{0,2,1:T(8,128)}, f32[4,192,4,64]{1,0,3,2:T(4,128)S(1)}) fusion(f32[4,192,4,64]{1,0,3,2:T(4,128)} %reshape.70, f32[4,192,4]{1,0,2:T(4,128)S(1)} %exponential_multiply_fusion), kind=kLoop, calls=%fused_computation.42 | loop fusion | flops 392192 | bytes 1589248 | tf_op jit(solution)/shard_map/reduce_sum | solution.py:43
  58.9 2.9 %fusion.3 = f32[4,4,64,128]{3,2,1,0:T(8,128)} fusion(f32[4,192,4,64]{1,0,3,2:T(4,128)S(1)} %get-tuple-element.219, bf16[4,192,4,128]{3,2,1,0:T(4,128)(2,1)} %reshape_reshape.12), kind=kOutput, calls=%fused_computation.13 | convolution fusion | flops 301989888 | bytes 2097152 | tf_op jit(solution)/shard_map/slhd,slhe->shde/dot_general | solution.py:42
  61.8 15.3 %all_to_all.24 = bf16[8,96,256]{2,1,0:T(8,128)(2,1)S(1)} all-to-all(bf16[8,96,256]{2,1,0:T(8,128)(2,1)} %bitcast.76), channel_id=1, replica_groups=mesh['gr'=2,'sp'=8,'tp'=2] {'sp'}, dimensions={0} | all-to-all | bytes 786432 | tf_op jit(solution)/shard_map/all_to_all | solution.py:72
  77.2 10.2 %all-to-all-start.1 = ((bf16[8,96,512]{2,1,0:T(8,128)(2,1)}), bf16[8,96,512]{2,1,0:T(8,128)(2,1)}, u32[]{:S(2)}, u32[]{:S(2)}) async-start(bf16[8,96,512]{2,1,0:T(8,128)(2,1)} %bitcast.74), calls=%async_computation.1 | async-start | bytes 1572864 | tf_op jit(solution)/shard_map/all_to_all | solution.py:79
  87.4 1.0 copy.40
  88.4 41.4 %all-gather.2 = f32[32,4,64]{2,1,0:T(4,128)S(1)} all-gather(f32[4,4,64]{2,1,0:T(4,128)S(1)} %copy.40), channel_id=4, replica_groups=mesh['gr'=2,'sp'=8,'tp'=2] {'sp'}, dimensions={0}, use_global_device_ids=true | all-gather | bytes 36864 | tf_op jit(solution)/shard_map/all_gather | solution.py:22
  129.8 0.6 slice.75
  130.4 1.3 slice.76
  131.7 0.7 reshape.67
  132.4 0.7 reshape.101
  133.1 26.5 %all-gather.5 = f32[8,4,4]{2,1,0:T(4,128)S(1)} all-gather(f32[1,4,4]{2,1,0:T(4,128)S(1)} %bitcast.82), channel_id=5, replica_groups=mesh['gr'=2,'sp'=8,'tp'=2] {'sp'}, dimensions={0}, use_global_device_ids=true | all-gather | bytes 576 | tf_op jit(solution)/shard_map/all_gather | solution.py:22
  159.6 0.6 slice.73
  160.2 0.7 slice_bitcast_fusion
  160.9 1.9 slice.69
  162.8 4.4 %slice.74 = f32[28,4,64,128]{3,2,1,0:T(8,128)} slice(f32[32,4,64,128]{3,2,1,0:T(8,128)} %all-gather.8.cloned.1.call-done), slice={[4:32], [0:4], [0:64], [0:128]} | slice | bytes 7340032 | tf_op jit(solution)/shard_map/slice | solution.py:24
  167.1 30.0 %while.32 = (s32[]{:T(128)}, f32[4,4,64,128]{3,2,1,0:T(8,128)}, f32[4,4,64]{2,1,0:T(4,128)S(1)}, f32[4,4]{1,0:T(4,128)S(1)}, f32[4,4]{1,0:T(4,128)S(1)}, /*index...) while((s32[]{:T(128)}, f32[4,4,64,128]{3,2,1,0:T(8,128)}, ...), condition=%wide.region_8.9_spmd, body=%wide.region_7.8_spmd.sunk | while | flops 396354 | bytes 1586173 | solution.py:25
  167.1 0.7 subtract_exponential_fusion.3
  167.8 0.7 bitcast_add_fusion.2
  168.5 2.1 %fusion.27 = f32[4,4,64,128]{3,2,1,0:T(8,128)} fusion(f32[7,4,4,64,128]{4,3,2,1,0:T(8,128)} %get-tuple-element.362, s32[]{:T(128)S(6)} %copy.64, f32[4,4,64,128]{3,2,1,0:T(8,128)} %get-tuple-element.347, f32[4,4]{1,0:T(4,128)S(1)} %get-tuple-element.305, f32[4,4]{1,0:T(4,128)S(1)} %get-tuple-element.306), kind=kLoop, calls=%fused_computation.1.clone.1 | loop fusion | flops 393216 | bytes 1572996 | tf_op jit(solution)/shard_map/while/body/eval_jaxpr/add | solution.py:50
  170.6 0.8 fusion.28
  171.4 0.7 subtract_exponential_fusion.3
  172.1 0.7 bitcast_add_fusion.2
  172.8 2.1 %fusion.27 = f32[4,4,64,128]{3,2,1,0:T(8,128)} fusion(f32[7,4,4,64,128]{4,3,2,1,0:T(8,128)} %get-tuple-element.362, s32[]{:T(128)S(6)} %copy.64, f32[4,4,64,128]{3,2,1,0:T(8,128)} %get-tuple-element.347, f32[4,4]{1,0:T(4,128)S(1)} %get-tuple-element.305, f32[4,4]{1,0:T(4,128)S(1)} %get-tuple-element.306), kind=kLoop, calls=%fused_computation.1.clone.1 | loop fusion | flops 393216 | bytes 1572996 | tf_op jit(solution)/shard_map/while/body/eval_jaxpr/add | solution.py:50
  174.9 0.8 fusion.28
  175.7 0.7 subtract_exponential_fusion.3
  176.4 0.7 bitcast_add_fusion.2
  177.1 2.1 %fusion.27 = f32[4,4,64,128]{3,2,1,0:T(8,128)} fusion(f32[7,4,4,64,128]{4,3,2,1,0:T(8,128)} %get-tuple-element.362, s32[]{:T(128)S(6)} %copy.64, f32[4,4,64,128]{3,2,1,0:T(8,128)} %get-tuple-element.347, f32[4,4]{1,0:T(4,128)S(1)} %get-tuple-element.305, f32[4,4]{1,0:T(4,128)S(1)} %get-tuple-element.306), kind=kLoop, calls=%fused_computation.1.clone.1 | loop fusion | flops 393216 | bytes 1572996 | tf_op jit(solution)/shard_map/while/body/eval_jaxpr/add | solution.py:50
  179.2 0.8 fusion.28
  180.0 0.7 subtract_exponential_fusion.3
  180.7 0.7 bitcast_add_fusion.2
  181.4 2.1 %fusion.27 = f32[4,4,64,128]{3,2,1,0:T(8,128)} fusion(f32[7,4,4,64,128]{4,3,2,1,0:T(8,128)} %get-tuple-element.362, s32[]{:T(128)S(6)} %copy.64, f32[4,4,64,128]{3,2,1,0:T(8,128)} %get-tuple-element.347, f32[4,4]{1,0:T(4,128)S(1)} %get-tuple-element.305, f32[4,4]{1,0:T(4,128)S(1)} %get-tuple-element.306), kind=kLoop, calls=%fused_computation.1.clone.1 | loop fusion | flops 393216 | bytes 1572996 | tf_op jit(solution)/shard_map/while/body/eval_jaxpr/add | solution.py:50
  183.5 0.8 fusion.28
  184.3 0.7 subtract_exponential_fusion.3
  185.0 0.7 bitcast_add_fusion.2
  185.7 2.1 %fusion.27 = f32[4,4,64,128]{3,2,1,0:T(8,128)} fusion(f32[7,4,4,64,128]{4,3,2,1,0:T(8,128)} %get-tuple-element.362, s32[]{:T(128)S(6)} %copy.64, f32[4,4,64,128]{3,2,1,0:T(8,128)} %get-tuple-element.347, f32[4,4]{1,0:T(4,128)S(1)} %get-tuple-element.305, f32[4,4]{1,0:T(4,128)S(1)} %get-tuple-element.306), kind=kLoop, calls=%fused_computation.1.clone.1 | loop fusion | flops 393216 | bytes 1572996 | tf_op jit(solution)/shard_map/while/body/eval_jaxpr/add | solution.py:50
  187.8 0.8 fusion.28
  188.6 0.7 subtract_exponential_fusion.3
  189.3 0.7 bitcast_add_fusion.2
  189.9 2.1 %fusion.27 = f32[4,4,64,128]{3,2,1,0:T(8,128)} fusion(f32[7,4,4,64,128]{4,3,2,1,0:T(8,128)} %get-tuple-element.362, s32[]{:T(128)S(6)} %copy.64, f32[4,4,64,128]{3,2,1,0:T(8,128)} %get-tuple-element.347, f32[4,4]{1,0:T(4,128)S(1)} %get-tuple-element.305, f32[4,4]{1,0:T(4,128)S(1)} %get-tuple-element.306), kind=kLoop, calls=%fused_computation.1.clone.1 | loop fusion | flops 393216 | bytes 1572996 | tf_op jit(solution)/shard_map/while/body/eval_jaxpr/add | solution.py:50
  192.1 0.8 fusion.28
  192.8 0.7 subtract_exponential_fusion.3
  193.5 0.7 bitcast_add_fusion.2
  194.2 2.1 %fusion.27 = f32[4,4,64,128]{3,2,1,0:T(8,128)} fusion(f32[7,4,4,64,128]{4,3,2,1,0:T(8,128)} %get-tuple-element.362, s32[]{:T(128)S(6)} %copy.64, f32[4,4,64,128]{3,2,1,0:T(8,128)} %get-tuple-element.347, f32[4,4]{1,0:T(4,128)S(1)} %get-tuple-element.305, f32[4,4]{1,0:T(4,128)S(1)} %get-tuple-element.306), kind=kLoop, calls=%fused_computation.1.clone.1 | loop fusion | flops 393216 | bytes 1572996 | tf_op jit(solution)/shard_map/while/body/eval_jaxpr/add | solution.py:50
  196.3 0.8 fusion.28
  197.1 0.6 subtract_exponential_fusion.1
  197.7 1.1 broadcast_multiply_fusion.1
  198.9 1.3 multiply_reduce_fusion
  200.2 1.0 fusion.17
  201.4 0.6 copy.52
  202.0 0.7 copy.78
  202.7 2.1 copy.79
  (48 shorter events, 1.3 us)
Async XLA Ops:
  7.2 1.9 copy-start
  7.2 153.7 %all-gather.8.cloned.1.call-start = ((), (), s32[]{:S(2)}) async-start(), calls=%async_computation.2 | async-start | bytes 4718592 | tf_op jit(solution)/shard_map/all_gather | solution.py:22
  9.1 2.4 %copy-start.6 = (bf16[2048,512]{1,0:T(8,128)(2,1)S(1)}, bf16[2048,512]{1,0:T(8,128)(2,1)}, u32[]{:S(2)}) copy-start(bf16[2048,512]{1,0:T(8,128)(2,1)} %param.13) | copy-start | bytes 6291460
  11.4 2.7 %copy-start.2 = (bf16[768,256]{1,0:T(8,128)(2,1)}, bf16[768,256]{1,0:T(8,128)(2,1)S(1)}, u32[]{:S(2)}) copy-start(bf16[768,256]{1,0:T(8,128)(2,1)S(1)} %convolution_convert_fusion.1) | copy-start | bytes 1179652
  14.1 5.6 %copy-start.5 = (f32[4]{0:T(128)S(1)}, f32[4]{0:T(128)}, u32[]{:S(2)}) copy-start(f32[4]{0:T(128)} %param.16) | copy-start | bytes 52
  53.8 8.0 %copy-start.3 = (f32[8,4,4]{2,1,0:T(4,128)}, f32[8,4,4]{2,1,0:T(4,128)S(1)}, u32[]{:S(2)}) copy-start(f32[8,4,4]{2,1,0:T(4,128)S(1)} %get-tuple-element.384) | copy-start | bytes 1540
  58.9 72.8 %copy-start.4 = (bf16[4,256]{1,0:T(4,128)(2,1)S(1)}, bf16[4,256]{1,0:T(4,128)(2,1)}, u32[]{:S(2)}) copy-start(bf16[4,256]{1,0:T(4,128)(2,1)} %param.17) | copy-start | bytes 6148
  77.2 83.7 %all-to-all-start.1 = ((bf16[8,96,512]{2,1,0:T(8,128)(2,1)}), bf16[8,96,512]{2,1,0:T(8,128)(2,1)}, u32[]{:S(2)}, u32[]{:S(2)}) async-start(bf16[8,96,512]{2,1,0:T(8,128)(2,1)} %bitcast.74), calls=%async_computation.1 | async-start | bytes 1572864 | tf_op jit(solution)/shard_map/all_to_all | solution.py:79
  198.9 5.9 %copy-start.1 = (f32[4,4,64,128]{3,2,1,0:T(8,128)}, f32[4,4,64,128]{3,2,1,0:T(8,128)S(1)}, u32[]{:S(2)}) copy-start(f32[4,4,64,128]{3,2,1,0:T(8,128)S(1)} %broadcast_multiply_fusion.1) | copy-start | bytes 1572868
Sparse Core Ops, SparseCore 0:
  61.9 87.9 all-gather.7
where the time goes:
time: 213 us; the launch traced here: 212 us
  blocking collectives  111 us (52%)
  other arithmetic  40.9 us (19%)
  local copies, waits for them, and re-layouts  24.3 us (11%)
  between operations  14.2 us (7%)
  matrix products  10.6 us (5%)
  starting transfers between devices  10.2 us (5%)
    all_gather x2, blocking collectives, merged(): pieces = jax.tree.map(lambda part: lax.all_gather(part, axis), value)  67.9 us
    all_gather x1, blocking collectives, carried_in(): everything = lax.all_gather(array, axis)  27.9 us
    all_to_all x1, blocking collectives, local(): lax.all_to_all(keys3.reshape(seqs * pieces, sub, heads * kdim), 'sp', spl...  15.3 us
    add x7, other arithmetic, merge_states(): first[0] * left[..., None, None] + second[0] * right[..., None, None]  14.8 us
    all_to_all x1, starting transfers between devices, local(): lax.all_to_all(values3.reshape(seqs * pieces, sub, heads * vdim), 'sp', s...  10.2 us
    slice x4, local copies, waits for them, and re-layouts, merged(): tail = jax.tree.map(lambda part: part[1:], pieces)  6.89 us
    add x7, other arithmetic, merge_states(): normal = first[1] * left[..., None] + second[1] * right[..., None]  5.45 us
    unnamed x17, local copies, waits for them, and re-layouts  5.28 us
  transfers between devices with their start and end apart: 2, of which 0 were waited for; matrix products, arithmetic and copies ran while one was open for 3% of the time, Pallas kernels for 0%

commit v1 on v0

--- a/solution.py
+++ b/solution.py
@@ -2,6 +2,12 @@
 import jax.numpy as jnp
 from jax import lax
 from jax.sharding import PartitionSpec as P
+
+
+def exchange_blocks(x, axis, split, join):
+    cells = jnp.split(x, lax.axis_size(axis), axis=split)
+    received = lax.all_to_all(jnp.stack(cells), axis, 0, 0)
+    return jnp.concatenate(received, axis=join)
 
 
 def carried_in(array, axis, combine, identity):
@@ -69,13 +75,7 @@
     keys3 = keys.reshape(seqs, span, heads * kdim)
     values3 = values.reshape(seqs, span, heads * vdim)
     key_cache, value_cache = (
-        lax.all_to_all(
-            keys3.reshape(seqs * pieces, sub, heads * kdim),
-            "sp",
-            split_axis=0,
-            concat_axis=1,
-            tiled=True,
-        ),
+        exchange_blocks(keys3.reshape(seqs * pieces, sub, heads * kdim), "sp", 0, 1),
         lax.all_to_all(
             values3.reshape(seqs * pieces, sub, heads * vdim),
             "sp",

time: 213 us -> 252 us (1.18)
  other arithmetic: 40.9 us -> 61.9 us
  local copies, waits for them, and re-layouts: 24.3 us -> 40.5 us
    select_n x8, other arithmetic: 0.12 us -> 10.2 us  [step(): return jnp.where(reached, new, before)]
    another operation x3, other arithmetic: 4.93 us -> 11.3 us
    another operation x4 -> x5, local copies, waits for them, and re-layouts: 0.15 us -> 4.65 us
    reshape x2, local copies, waits for them, and re-layouts: 0.03 us -> 2.67 us
    slice x2, local copies, waits for them, and re-layouts: 0.21 us -> 2.84 us
    unnamed x17 -> x26, local copies, waits for them, and re-layouts: 5.28 us -> 5.9 us
  transfers between devices with their start and end apart: 2 -> 2, of which waited for: 0 -> 0; matrix products, arithmetic and copies ran while one was open for 3% -> 2% of each run, Pallas kernels for 0% -> 0%
where the time goes in v1:
time: 252 us; the launch traced here: 249 us
  blocking collectives  112 us (44%)
  other arithmetic  61.9 us (25%)
  local copies, waits for them, and re-layouts  40.5 us (16%)
  between operations  14.2 us (6%)
  matrix products  10.6 us (4%)
  starting transfers between devices  10.1 us (4%)
    all_gather x2, blocking collectives, merged(): pieces = jax.tree.map(lambda part: lax.all_gather(part, axis), value)  68.2 us
    all_gather x1, blocking collectives, carried_in(): everything = lax.all_gather(array, axis)  29 us
    add x7, other arithmetic, merge_states(): first[0] * left[..., None, None] + second[0] * right[..., None, None]  14.8 us
    all_to_all x1, blocking collectives, exchange_blocks(): received = lax.all_to_all(jnp.stack(cells), axis, 0, 0)  14.6 us
    another operation x3, other arithmetic  11.3 us
    select_n x8, other arithmetic, step(): return jnp.where(reached, new, before)  10.2 us
    all_to_all x1, starting transfers between devices, local(): lax.all_to_all(values3.reshape(seqs * pieces, sub, heads * vdim), 'sp', s...  10.1 us
    slice x4, local copies, waits for them, and re-layouts, merged(): tail = jax.tree.map(lambda part: part[1:], pieces)  6.89 us
  transfers between devices with their start and end apart: 2, of which 0 were waited for; matrix products, arithmetic and copies ran while one was open for 2% of the time, Pallas kernels for 0%

profile of v1, /device:TPU:0, one launch (start us, length us, event | category | flops | bytes accessed | tf_op | source)
XLA Modules:
  0.0 249.2 jit_solution(16829823045683528822)
XLA Ops:
  7.2 1.8 copy-done
  9.1 2.4 convolution_convert_fusion.1
  11.4 2.7 %convolution_convert_fusion = bf16[768,512]{1,0:T(8,128)(2,1)} fusion(bf16[768,2048]{1,0:T(8,128)(2,1)S(1)} %bitcast.102, bf16[2048,512]{1,0:T(8,128)(2,1)S(1)} %copy-done.7), kind=kOutput, calls=%fused_computation.10 | convolution fusion | flops 1611005952 | bytes 6029312 | tf_op jit(solution)/shard_map/dot_general | solution.py:70
  14.1 1.1 copy.31
  15.2 2.8 %reshape.87 = f32[4,192,4,64]{1,0,3,2:T(4,128)} reshape(f32[768,256]{0,1:T(8,128)} %copy.31) | data formatting | bytes 1572864 | tf_op jit(solution)/shard_map/convert_element_type | solution.py:45
  18.1 1.6 convolution_bitcast_fusion
  20.4 0.8 reshape.83
  21.2 1.4 reshape.80
  22.6 1.4 reduce_sum.27
  24.0 1.3 pad.3
  25.3 1.3 reshape.81
  26.7 1.3 copy.34
  28.0 9.2 %reduce-window.6 = f32[4,4,2,128]{3,2,1,0:T(2,128)} reduce-window(f32[4,4,2,128]{3,2,1,0:T(2,128)} %copy.34, f32[]{:T(128)} %constant.71.clone.1), window={size=1x1x1x128 pad=0_0x0_0x0_0x127_0}, to_apply=%region_3.4 | reduce-window | flops 520192 | bytes 32772 | tf_op jit(solution)/shard_map/reduce-window
  37.2 1.4 slice.73
  38.6 1.4 copy.35
  41.3 1.4 copy.36
  42.7 1.4 broadcast_add_fusion
  44.1 1.3 reduce_window_sum.16
  45.4 1.3 copy.51
  46.8 1.3 copy.32
  48.1 29.0 %all-gather.4 = f32[8,4,4]{2,1,0:T(4,128)} all-gather(f32[1,4,4]{2,1,0:T(4,128)} %bitcast.113), channel_id=2, replica_groups=mesh['gr'=2,'sp'=8,'tp'=2] {'sp'}, dimensions={0}, use_global_device_ids=true | all-gather | bytes 576 | tf_op jit(solution)/shard_map/all_gather | solution.py:15
  77.1 10.2 %while.33 = (s32[]{:T(128)}, f32[4,4]{1,0:T(4,128)}, s32[]{:T(128)}, f32[8,4,4]{2,1,0:T(4,128)}, s32[]{:T(128)}, /*index=5*/s32[]{:T(128)}, s32[]{:T(128)}, s32[]{:T(128)}) while((s32[]{:T(128)}, f32[4,4]{1,0:T(4,128)}, s32[]{:T(128)}, f32[8,4,4]{2,1,0:T(4,128)}, s32[]{:T(128)}, /*index=5*/s32[]{:T(128)}, s32[]{:T(128)}, ...), condition=%wide.region_2.3_spmd.clone, body=%wide.region_1.2_spmd.clone.sunk | while | flops 56 | bytes 355 | solution.py:24
  77.1 1.3 add_select_fusion.2
  78.3 1.3 add_select_fusion.2
  79.6 1.3 add_select_fusion.2
  80.9 1.3 add_select_fusion.2
  82.1 1.3 add_select_fusion.2
  83.4 1.3 add_select_fusion.2
  84.7 1.3 add_select_fusion.2
  85.9 1.3 add_select_fusion.2
  87.2 1.3 copy.33
  89.2 0.9 fusion.22
  90.7 1.4 exponential_multiply_fusion
  92.1 2.4 reshape_reshape.9
  94.5 2.3 fusion.24
  96.8 2.9 %fusion.3 = f32[4,4,64,128]{3,2,1,0:T(8,128)} fusion(f32[4,192,4,64]{1,0,3,2:T(4,128)S(1)} %get-tuple-element.219, bf16[4,192,4,128]{3,2,1,0:T(4,128)(2,1)} %reshape_reshape.9), kind=kOutput, calls=%fused_computation.13 | convolution fusion | flops 301989888 | bytes 2097152 | tf_op jit(solution)/shard_map/slhd,slhe->shde/dot_general | solution.py:48
  99.9 14.6 %all_to_all.17 = bf16[8,1,96,256]{3,2,1,0:T(8,128)(2,1)S(1)} all-to-all(bf16[8,1,96,256]{3,2,1,0:T(8,128)(2,1)S(1)} %fusion.6), channel_id=1, replica_groups=mesh['gr'=2,'sp'=8,'tp'=2] {'sp'}, dimensions={0} | all-to-all | bytes 786432 | tf_op jit(solution)/shard_map/all_to_all | solution.py:9
  114.5 10.1 %all-to-all-start.1 = ((bf16[8,96,512]{2,1,0:T(8,128)(2,1)}), bf16[8,96,512]{2,1,0:T(8,128)(2,1)}, u32[]{:S(2)}, u32[]{:S(2)}) async-start(bf16[8,96,512]{2,1,0:T(8,128)(2,1)} %bitcast.105), calls=%async_computation.1 | async-start | bytes 1572864 | tf_op jit(solution)/shard_map/all_to_all | solution.py:79
  124.7 1.0 copy.40
  125.7 41.7 %all-gather.2 = f32[32,4,64]{2,1,0:T(4,128)S(1)} all-gather(f32[4,4,64]{2,1,0:T(4,128)S(1)} %copy.40), channel_id=4, replica_groups=mesh['gr'=2,'sp'=8,'tp'=2] {'sp'}, dimensions={0}, use_global_device_ids=true | all-gather | bytes 36864 | tf_op jit(solution)/shard_map/all_gather | solution.py:28
  168.0 1.3 slice.84
  170.7 26.5 %all-gather.5 = f32[8,4,4]{2,1,0:T(4,128)S(1)} all-gather(f32[1,4,4]{2,1,0:T(4,128)S(1)} %bitcast.112), channel_id=5, replica_groups=mesh['gr'=2,'sp'=8,'tp'=2] {'sp'}, dimensions={0}, use_global_device_ids=true | all-gather | bytes 576 | tf_op jit(solution)/shard_map/all_gather | solution.py:28
  198.5 1.9 slice.77
  200.3 4.4 %slice.82 = f32[28,4,64,128]{3,2,1,0:T(8,128)} slice(f32[32,4,64,128]{3,2,1,0:T(8,128)} %all-gather.8.cloned.1.call-done), slice={[4:32], [0:4], [0:64], [0:128]} | slice | bytes 7340032 | tf_op jit(solution)/shard_map/slice | solution.py:30
  204.7 30.0 %while.32 = (s32[]{:T(128)}, f32[4,4,64,128]{3,2,1,0:T(8,128)}, f32[4,4,64]{2,1,0:T(4,128)S(1)}, f32[4,4]{1,0:T(4,128)S(1)}, f32[4,4]{1,0:T(4,128)S(1)}, /*index...) while((s32[]{:T(128)}, f32[4,4,64,128]{3,2,1,0:T(8,128)}, ...), condition=%wide.region_8.9_spmd, body=%wide.region_7.8_spmd.sunk | while | flops 396354 | bytes 1586173 | solution.py:31
  206.1 2.1 fusion.35
  208.2 0.8 fusion.36
  210.4 2.1 fusion.35
  212.5 0.8 fusion.36
  214.6 2.1 fusion.35
  216.8 0.8 fusion.36
  218.9 2.1 fusion.35
  221.0 0.8 fusion.36
  223.2 2.1 fusion.35
  225.3 0.8 fusion.36
  227.5 2.1 fusion.35
  229.6 0.8 fusion.36
  231.8 2.1 fusion.35
  233.9 0.8 fusion.36
  235.3 1.1 broadcast_multiply_fusion.1
  236.5 1.4 multiply_reduce_fusion
  237.8 1.0 fusion.25
  239.6 0.7 copy.85
  240.3 2.1 copy.86
  (58 shorter events, 17.7 us)
Async XLA Ops:
  7.2 1.9 copy-start
  7.2 191.3 %all-gather.8.cloned.1.call-start = ((), (), s32[]{:S(2)}) async-start(), calls=%async_computation.2 | async-start | bytes 4718592 | tf_op jit(solution)/shard_map/all_gather | solution.py:28
  9.1 2.4 copy-start.7
  11.4 6.6 %copy-start.4 = (bf16[2048,4]{0,1:T(4,128)(2,1)S(1)}, bf16[2048,4]{0,1:T(4,128)(2,1)}, u32[]{:S(2)}) copy-start(bf16[2048,4]{0,1:T(4,128)(2,1)} %param.15) | copy-start | bytes 49156
  18.1 1.6 copy-start.6
  90.1 0.6 copy-start.2
  96.8 27.7 %copy-start.3 = (f32[4,4]{0,1:T(4,128)S(1)}, f32[4,4]{0,1:T(4,128)}, u32[]{:S(2)}) copy-start(f32[4,4]{0,1:T(4,128)} %copy-done.2) | copy-start | bytes 196
  96.8 72.5 %copy-start.5 = (bf16[4,256]{1,0:T(4,128)(2,1)S(1)}, bf16[4,256]{1,0:T(4,128)(2,1)}, u32[]{:S(2)}) copy-start(bf16[4,256]{1,0:T(4,128)(2,1)} %param.17) | copy-start | bytes 6148
  114.5 84.0 %all-to-all-start.1 = ((bf16[8,96,512]{2,1,0:T(8,128)(2,1)}), bf16[8,96,512]{2,1,0:T(8,128)(2,1)}, u32[]{:S(2)}, u32[]{:S(2)}) async-start(bf16[8,96,512]{2,1,0:T(8,128)(2,1)} %bitcast.105), calls=%async_computation.1 | async-start | bytes 1572864 | tf_op jit(solution)/shard_map/all_to_all | solution.py:79
  236.5 5.9 %copy-start.1 = (f32[4,4,64,128]{3,2,1,0:T(8,128)}, f32[4,4,64,128]{3,2,1,0:T(8,128)S(1)}, u32[]{:S(2)}) copy-start(f32[4,4,64,128]{3,2,1,0:T(8,128)S(1)} %broadcast_multiply_fusion.1) | copy-start | bytes 1572868
Sparse Core Ops, SparseCore 0:
  99.9 87.7 all-gather.7
